TPU v7x, 32 devices: a whole 2x2x4 slice. The times are simulated.
32 devices in a mesh: grp: 2 (over y), sp: 4 (over z), dp: 4 (over x, core).
Axes of the slice: x: 2, y: 2, z: 4, core: 2. Of those that a mesh axis runs over, the one named last changes fastest.
Arguments:
- tokens: bfloat16 [8, 512, 2048], P(('grp', 'dp'), 'sp'), parts along dimension 0, may hold values from -6 to 6
- forget_offset: float32 [8, 512], P(('grp', 'dp'), 'sp'), parts along dimension 0, may hold values from -1.2 to 1.2, as said below
- q_weight: bfloat16 [2048, 2048], P(None, 'dp'), may hold values from -0.125 to 0.125
- k_weight: bfloat16 [2048, 512], P(None, 'dp'), may hold values from -0.125 to 0.125
- v_weight: bfloat16 [2048, 512], P(None, 'dp'), may hold values from -0.125 to 0.125
- forget_weight: bfloat16 [2048, 16], replicated, may hold values from -0.125 to 0.125
- forget_bias: float32 [16], replicated, may hold values from 3 to 12
- score_gain: float32 [16], replicated, may hold values from 0.5 to 80
- out_gain: float32 [2048], replicated, may hold values from 0.1 to 1.9
Outputs:
- attended: bfloat16 [8, 512, 2048], P(('grp', 'dp'), 'sp'), parts along dimension 0
There are 2 independent parts, one for each index of `grp`. A program takes and returns all parts, laid end to end along the dimension named above; an argument that names none is the same for every part. Nothing has to cross between parts.
Inputs may be any that keep to these rules, and one draw needn't show every extreme that they name: `forget_offset`: constant over aligned spans of 64 positions.
All inputs are finite; a program needn't handle non-finite values.
Results may differ from a plain program's by a relative error of at most 0.0085.
The roundings to bfloat16 on the way count: a program that leaves them out, or rounds other values in their place, can miss the bound.
Values may be sent and summed in bfloat16 or wider, within the bound.
A program may use at most 128 MiB of HBM per device.

v0:
```python
import jax
import jax.numpy as jnp
from jax import lax
from jax.sharding import PartitionSpec as P

NEG = -1e30
QK_FLOOR = 0.1
OUT_FLOOR = 0.001


def head_norm(vectors, floor):
    return vectors * lax.rsqrt(jnp.mean(vectors * vectors, axis=-1, keepdims=True) + floor)


def local(
    tokens,
    forget_offset,
    q_weight,
    k_weight,
    v_weight,
    forget_weight,
    forget_bias,
    score_gain,
    out_gain,
):
    own_rows = tokens[0]
    tok_count = own_rows.shape[0]
    head_count = forget_bias.shape[0]
    head_dim = out_gain.shape[0] // head_count
    kv_heads = k_weight.shape[1] * lax.axis_size("dp") // head_dim
    spread = lax.axis_size("sp")
    local_heads = head_count // spread
    local_kv = max(1, kv_heads // spread)
    group_size = local_heads // local_kv
    everyone = lax.all_gather(tokens, "dp", axis=0, tiled=True)
    seq_count = everyone.shape[0]
    flat_rows = everyone.reshape(seq_count * tok_count, everyone.shape[2])
    query_cols = (
        jnp.dot(flat_rows, q_weight, preferred_element_type=jnp.float32)
        .astype(jnp.bfloat16)
        .reshape(seq_count, tok_count, -1)
    )
    key_cols = (
        jnp.dot(flat_rows, k_weight, preferred_element_type=jnp.float32)
        .astype(jnp.bfloat16)
        .reshape(seq_count, tok_count, -1)
    )
    value_cols = (
        jnp.dot(flat_rows, v_weight, preferred_element_type=jnp.float32)
        .astype(jnp.bfloat16)
        .reshape(seq_count, tok_count, -1)
    )
    query_mine, key_mine, value_mine = (
        lax.all_to_all(query_cols, "dp", split_axis=0, concat_axis=2, tiled=True),
        lax.all_to_all(key_cols, "dp", split_axis=0, concat_axis=2, tiled=True),
        lax.all_to_all(value_cols, "dp", split_axis=0, concat_axis=2, tiled=True),
    )
    queries = query_mine[0]
    keys_proj = key_mine[0]
    values_proj = value_mine[0]
    forget_input = (
        jnp.dot(own_rows, forget_weight, preferred_element_type=jnp.float32)
        + forget_offset[0][:, None]
    ).astype(jnp.bfloat16)
    query_send = queries.reshape(tok_count, spread, local_heads, head_dim)
    forget_send = forget_input.reshape(tok_count, spread, local_heads)
    if kv_heads >= spread:
        key_send = keys_proj.reshape(tok_count, spread, local_kv, head_dim)
        value_send = values_proj.reshape(tok_count, spread, local_kv, head_dim)
    else:
        copies = spread // kv_heads
        key_send = jnp.broadcast_to(
            keys_proj.reshape(tok_count, kv_heads, 1, head_dim),
            (tok_count, kv_heads, copies, head_dim),
        ).reshape(tok_count, spread, 1, head_dim)
        value_send = jnp.broadcast_to(
            values_proj.reshape(tok_count, kv_heads, 1, head_dim),
            (tok_count, kv_heads, copies, head_dim),
        ).reshape(tok_count, spread, 1, head_dim)
    query_head, forget_head, key_head, value_head = (
        lax.all_to_all(query_send, "sp", split_axis=1, concat_axis=0, tiled=True),
        lax.all_to_all(forget_send, "sp", split_axis=1, concat_axis=0, tiled=True),
        lax.all_to_all(key_send, "sp", split_axis=1, concat_axis=0, tiled=True),
        lax.all_to_all(value_send, "sp", split_axis=1, concat_axis=0, tiled=True),
    )
    length = query_head.shape[0]
    first_head = lax.axis_index("sp") * local_heads
    bias_local = lax.dynamic_slice_in_dim(forget_bias, first_head, local_heads, 0)
    gain_local = lax.dynamic_slice_in_dim(score_gain, first_head, local_heads, 0)
    norm_local = lax.dynamic_slice_in_dim(
        out_gain, first_head * head_dim, local_heads * head_dim, 0
    )
    log_gate = jax.nn.log_sigmoid(
        forget_head.reshape(length, local_heads).astype(jnp.float32) + bias_local[None, :]
    )
    cumulative = jnp.cumsum(log_gate, axis=0).reshape(length, local_kv, group_size)
    query_unit = head_norm(query_head.astype(jnp.float32), QK_FLOOR).astype(jnp.bfloat16)
    key_unit = head_norm(
        key_head.reshape(length, local_kv, head_dim).astype(jnp.float32), QK_FLOOR
    ).astype(jnp.bfloat16)
    value_heads = value_head.reshape(length, local_kv, head_dim)
    factor = (gain_local * head_dim ** (-0.5)).reshape(local_kv, group_size)
    out_gains = norm_local.reshape(local_kv, group_size, head_dim)
    key_totals = jnp.transpose(cumulative, (1, 2, 0))
    span_rows = 512
    positions = jnp.arange(length, dtype=jnp.int32)

    def attend_block(block_index):
        first = block_index * span_rows
        query_block = lax.dynamic_slice_in_dim(query_unit, first, span_rows, 0)
        query_totals = lax.dynamic_slice_in_dim(cumulative, first, span_rows, 0)
        scores = jnp.einsum(
            "qkgd,skd->kgqs", query_block, key_unit, preferred_element_type=jnp.float32
        )
        scores = (
            scores * factor[:, :, None, None]
            + jnp.transpose(query_totals, (1, 2, 0))[..., None]
            - key_totals[:, :, None, :]
        )
        allowed = positions[None, :] <= (first + jnp.arange(span_rows, dtype=jnp.int32))[:, None]
        scores = jnp.where(allowed[None, None], scores, NEG)
        row_peak = jnp.max(scores, axis=-1, keepdims=True)
        exponent = jnp.exp(scores - row_peak)
        weights = (exponent / jnp.sum(exponent, axis=-1, keepdims=True)).astype(jnp.bfloat16)
        mixed = jnp.einsum(
            "kgqs,skd->qkgd", weights, value_heads, preferred_element_type=jnp.float32
        )
        return (head_norm(mixed, OUT_FLOOR) * out_gains).astype(jnp.bfloat16)

    outputs = lax.map(attend_block, jnp.arange(length // span_rows, dtype=jnp.int32))
    outputs = outputs.reshape(length, local_heads, head_dim)
    back_rows = lax.all_to_all(outputs, "sp", split_axis=0, concat_axis=1, tiled=True)
    return back_rows.reshape(1, tok_count, head_count * head_dim)


def solution(mesh):
    in_specs = (
        P(("grp", "dp"), "sp", None),
        P(("grp", "dp"), "sp"),
        P(None, "dp"),
        P(None, "dp"),
        P(None, "dp"),
        P(),
        P(),
        P(),
        P(),
    )
    out_specs = P(("grp", "dp"), "sp", None)
    return jax.shard_map(local, mesh=mesh, in_specs=in_specs, out_specs=out_specs, check_vma=False)
```

profile of v0, /device:TPU:0, one launch (start us, length us, event | category | flops | bytes accessed | tf_op | source)
XLA Modules:
  0.0 133.0 jit_solution(4874085769551353659)
XLA Ops:
  6.5 0.0 copy-start
  6.5 0.0 all-gather.2.cloned.1.call-start
  6.5 0.7 all-gather.2.cloned.1.call-update
  7.3 2.0 %fusion.10 = bf16[128,16]{0,1:T(8,128)(2,1)} fusion(bf16[2048,16]{0,1:T(8,128)(2,1)} %param.14, bf16[1,128,2048]{2,1,0:T(8,128)(2,1)} %param.9, f32[128]{0:T(128)} %bitcast.174), kind=kOutput, calls=%fused_computation.16 | convolution fusion | flops 8392704 | bytes 594432 | tf_op jit(solution)/shard_map/dot_general | solution.py:62
  9.2 6.3 %all-to-all-start.6 = ((bf16[128,4,4]{0,2,1:T(4,128)(2,1)}), bf16[128,4,4]{0,2,1:T(4,128)(2,1)S(1)}, u32[]{:S(2)}, u32[]{:S(2)}) async-start(bf16[128,4,4]{0,2,1:T(4,128)(2,1)} %bitcast.32), calls=%async_computation.6 | async-start | bytes 8192 | tf_op jit(solution)/shard_map/all_to_all | solution.py:82
  15.6 18.6 %all-gather.2.cloned.1.call-done = bf16[4,128,2048]{2,1,0:T(8,128)(2,1)} async-done(((bf16[1,128,2048]{2,1,0:T(8,128)(2,1)}), bf16[4,128,2048]{2,1,0:T(8,128)(2,1)}) %all-gather.2.cloned.1.call-update) | async-done | bytes 2097168 | tf_op jit(solution)/shard_map/all_gather | solution.py:35
  34.2 3.0 %convolution_convert_fusion.2 = bf16[512,128]{1,0:T(8,128)(2,1)} fusion(bf16[512,2048]{1,0:T(8,128)(2,1)} %bitcast.161, bf16[2048,128]{1,0:T(8,128)(2,1)} %param.13), kind=kOutput, calls=%fused_computation.14 | convolution fusion | flops 268500992 | bytes 2752512 | tf_op jit(solution)/shard_map/dot_general | solution.py:49
  37.2 0.0 all-to-all-done.6
  37.3 4.0 %all-to-all-start = ((bf16[4,128,128]{2,1,0:T(8,128)(2,1)}), bf16[4,128,128]{2,1,0:T(8,128)(2,1)}, u32[]{:S(2)}, u32[]{:S(2)}) async-start(bf16[4,128,128]{2,1,0:T(8,128)(2,1)} %bitcast.1), calls=%async_computation | async-start | bytes 262144 | tf_op jit(solution)/shard_map/all_to_all | solution.py:56
  41.2 3.0 %convolution_convert_fusion.1 = bf16[512,128]{1,0:T(8,128)(2,1)} fusion(bf16[512,2048]{1,0:T(8,128)(2,1)} %bitcast.162, bf16[2048,128]{1,0:T(8,128)(2,1)S(1)} %copy-done.2), kind=kOutput, calls=%fused_computation.13 | convolution fusion | flops 268500992 | bytes 2752512 | tf_op jit(solution)/shard_map/dot_general | solution.py:44
  44.2 1.7 %all-to-all-done = bf16[4,128,128]{2,1,0:T(8,128)(2,1)} async-done(((bf16[4,128,128]{2,1,0:T(8,128)(2,1)}), bf16[4,128,128]{2,1,0:T(8,128)(2,1)}, u32[]{:S(2)}, u32[]{:S(2)}) %all-to-all-start) | async-done | bytes 131104 | tf_op jit(solution)/shard_map/all_to_all | solution.py:56
  45.9 4.0 %all-to-all-start.2 = ((bf16[4,128,128]{2,1,0:T(8,128)(2,1)}), bf16[4,128,128]{2,1,0:T(8,128)(2,1)}, u32[]{:S(2)}, u32[]{:S(2)}) async-start(bf16[4,128,128]{2,1,0:T(8,128)(2,1)} %bitcast.9), calls=%async_computation.2 | async-start | bytes 262144 | tf_op jit(solution)/shard_map/all_to_all | solution.py:55
  49.9 0.0 copy-start.3
  49.9 0.0 copy-start.4
  49.9 2.8 %convolution_convert_fusion = bf16[512,512]{1,0:T(8,128)(2,1)S(1)} fusion(bf16[512,2048]{1,0:T(8,128)(2,1)} %bitcast.163, bf16[2048,512]{1,0:T(8,128)(2,1)S(1)} %copy-done), kind=kOutput, calls=%fused_computation.12 | convolution fusion | flops 1074003968 | bytes 4718592 | tf_op jit(solution)/shard_map/dot_general | solution.py:39
  52.7 1.0 copy.23
  53.7 0.8 all-to-all-done.2
  54.5 3.5 %all-to-all-start.4 = ((bf16[4,128,512]{1,2,0:T(8,128)(2,1)}), bf16[4,128,512]{1,2,0:T(8,128)(2,1)S(1)}, u32[]{:S(2)}, u32[]{:S(2)}) async-start(bf16[4,128,512]{1,2,0:T(8,128)(2,1)} %copy.23), calls=%async_computation.4 | async-start | bytes 1048576 | tf_op jit(solution)/shard_map/all_to_all | solution.py:54
  58.0 0.0 copy-done.3
  58.0 0.1 dynamic_slice.17
  58.1 0.8 dynamic-slice_bitcast_fusion
  58.8 7.9 %all-to-all-done.4 = bf16[4,128,512]{1,2,0:T(8,128)(2,1)S(1)} async-done(((bf16[4,128,512]{1,2,0:T(8,128)(2,1)}), bf16[4,128,512]{1,2,0:T(8,128)(2,1)S(1)}, u32[]{:S(2)}, u32[]{:S(2)}) %all-to-all-start.4) | async-done | bytes 524320 | tf_op jit(solution)/shard_map/all_to_all | solution.py:54
  66.8 4.6 %all-to-all-start.3 = ((bf16[128,4,1,128]{3,0,2,1:T(8,128)(2,1)}), bf16[128,4,1,128]{3,0,2,1:T(8,128)(2,1)S(1)}, u32[]{:S(2)}, u32[]{:S(2)}) async-start(bf16[128,4,1,128]{3,0,2,1:T(8,128)(2,1)} %bitcast.12), calls=%async_computation.3 | async-start | bytes 262144 | tf_op jit(solution)/shard_map/all_to_all | solution.py:83
  71.4 0.1 dynamic-slice_multiply_fusion
  71.4 0.1 iota_compare_fusion
  71.5 1.0 copy.24
  72.5 4.8 %all-to-all-done.3 = bf16[128,4,1,128]{3,0,2,1:T(8,128)(2,1)S(1)} async-done(((bf16[128,4,1,128]{3,0,2,1:T(8,128)(2,1)}), bf16[128,4,1,128]{3,0,2,1:T(8,128)(2,1)S(1)}, u32[]{:S(2)}, u32[]{:S(2)}) %all-to-all-start.3) | async-done | bytes 131104 | tf_op jit(solution)/shard_map/all_to_all | solution.py:83
  77.3 3.5 %all-to-all-start.5 = ((bf16[128,4,4,128]{3,0,2,1:T(8,128)(2,1)}), bf16[128,4,4,128]{3,0,2,1:T(8,128)(2,1)S(1)}, u32[]{:S(2)}, u32[]{:S(2)}) async-start(bf16[128,4,4,128]{3,0,2,1:T(8,128)(2,1)} %copy.24), calls=%async_computation.5 | async-start | bytes 1048576 | tf_op jit(solution)/shard_map/all_to_all | solution.py:81
  80.8 0.1 fusion.22
  80.9 1.2 reduce-window.6
  82.2 0.2 slice_reduce_fusion
  82.3 0.2 reduce-window.9
  82.5 0.1 add_bitcast_fusion
  82.6 0.1 multiply_reduce_fusion.1
  82.8 11.1 %all-to-all-done.5 = bf16[128,4,4,128]{3,0,2,1:T(8,128)(2,1)S(1)} async-done(((bf16[128,4,4,128]{3,0,2,1:T(8,128)(2,1)}), bf16[128,4,4,128]{3,0,2,1:T(8,128)(2,1)S(1)}, u32[]{:S(2)}, u32[]{:S(2)}) %all-to-all-start.5) | async-done | bytes 524320 | tf_op jit(solution)/shard_map/all_to_all | solution.py:81
  93.9 3.3 %all-to-all-start.1 = ((bf16[128,4,1,128]{3,0,2,1:T(8,128)(2,1)}), bf16[128,4,1,128]{3,0,2,1:T(8,128)(2,1)S(1)}, u32[]{:S(2)}, u32[]{:S(2)}) async-start(bf16[128,4,1,128]{3,0,2,1:T(8,128)(2,1)} %bitcast.4), calls=%async_computation.1 | async-start | bytes 262144 | tf_op jit(solution)/shard_map/all_to_all | solution.py:84
  97.2 0.4 fusion.13
  97.6 0.3 fusion.14
  97.9 1.3 fusion.3
  99.2 1.9 %copy-done.1 = f32[512,512,4]{1,0,2:T(8,128)} copy-done((f32[512,512,4]{1,0,2:T(8,128)}, f32[512,512,4]{1,0,2:T(8,128)S(1)}, u32[]{:S(2)}) %copy-start.1) | copy-done | bytes 4194328
  101.2 1.4 %fusion.2 = f32[4,512]{1,0:T(4,128)S(1)} fusion(f32[512,512,4]{1,0,2:T(8,128)S(1)} %get-tuple-element.24, f32[4,512]{1,0:T(4,128)S(1)} %get-tuple-element.23, f32[4,512]{1,0:T(4,128)S(1)} %bitcast.171, f32[4]{0:T(128)S(1)} %dynamic-slice_multiply_fusion, pred[512,512]{0,1:T(8,128)(4,1)S(1)} %iota_compare_fusion), kind=kLoop, calls=%fused_computation.6 | loop fusion | flops 6289408 | bytes 4481040 | tf_op jit(solution)/shard_map/while/body/eval_jaxpr/reduce_sum | solution.py:124
  102.6 0.5 all-to-all-done.1
  103.1 3.7 %multiply_reduce_fusion = (f32[512,4]{0,1:T(4,128)S(1)}, f32[512,1,4,128]{0,3,2,1:T(8,128)S(1)}) fusion(bf16[512,128,1]{1,0,2:T(8,128)(2,1)S(1)} %bitcast.169, f32[4,512]{1,0:T(4,128)S(1)} %fusion.2, f32[4,512]{1,0:T(4,128)S(1)} %get-tuple-element.23, f32[4,512]{1,0:T(4,128)S(1)} %bitcast.172, f32[4]{0:T(128)S(1)} %dynamic-slice_multiply_fusion, ...), kind=kOutput, calls=%fused_computation.23 | convolution fusion | flops 276297728 | bytes 5668880 | tf_op jit(solution)/shard_map/while/body/eval_jaxpr/kgqs,skd->qkgd/dot_general | solution.py:125
  106.9 0.2 fusion.15
  107.0 0.3 copy.27
  107.4 17.5 %all_to_all.102 = bf16[512,4,128]{2,1,0:T(4,128)(2,1)S(1)} all-to-all(bf16[512,4,128]{2,1,0:T(4,128)(2,1)S(1)} %copy.27), channel_id=1, replica_groups=mesh['grp'=2,'sp'=4,'dp'=4] {'sp'}, dimensions={0} | all-to-all | bytes 1048576 | tf_op jit(solution)/shard_map/all_to_all | solution.py:132
  124.8 0.2 copy.28
  125.0 1.2 reshape.234
  (11 shorter events, 0.1 us)
Async XLA Ops:
  6.5 43.3 %copy-start = (bf16[2048,512]{1,0:T(8,128)(2,1)S(1)}, bf16[2048,512]{1,0:T(8,128)(2,1)}, u32[]{:S(2)}) copy-start(bf16[2048,512]{1,0:T(8,128)(2,1)} %param.11) | copy-start | bytes 6291460
  6.5 34.7 %copy-start.2 = (bf16[2048,128]{1,0:T(8,128)(2,1)S(1)}, bf16[2048,128]{1,0:T(8,128)(2,1)}, u32[]{:S(2)}) copy-start(bf16[2048,128]{1,0:T(8,128)(2,1)} %param.12) | copy-start | bytes 1572868
  6.5 27.7 %all-gather.2.cloned.1.call-start = ((), (), s32[]{:S(2)}) async-start(), calls=%async_computation.8 | async-start | bytes 2621440 | tf_op jit(solution)/shard_map/all_gather | solution.py:35
  9.2 28.0 %all-to-all-start.6 = ((bf16[128,4,4]{0,2,1:T(4,128)(2,1)}), bf16[128,4,4]{0,2,1:T(4,128)(2,1)S(1)}, u32[]{:S(2)}, u32[]{:S(2)}) async-start(bf16[128,4,4]{0,2,1:T(4,128)(2,1)} %bitcast.32), calls=%async_computation.6 | async-start | bytes 8192 | tf_op jit(solution)/shard_map/all_to_all | solution.py:82
  37.3 8.6 %all-to-all-start = ((bf16[4,128,128]{2,1,0:T(8,128)(2,1)}), bf16[4,128,128]{2,1,0:T(8,128)(2,1)}, u32[]{:S(2)}, u32[]{:S(2)}) async-start(bf16[4,128,128]{2,1,0:T(8,128)(2,1)} %bitcast.1), calls=%async_computation | async-start | bytes 262144 | tf_op jit(solution)/shard_map/all_to_all | solution.py:56
  45.9 8.6 %all-to-all-start.2 = ((bf16[4,128,128]{2,1,0:T(8,128)(2,1)}), bf16[4,128,128]{2,1,0:T(8,128)(2,1)}, u32[]{:S(2)}, u32[]{:S(2)}) async-start(bf16[4,128,128]{2,1,0:T(8,128)(2,1)} %bitcast.9), calls=%async_computation.2 | async-start | bytes 262144 | tf_op jit(solution)/shard_map/all_to_all | solution.py:55
  49.9 8.1 %copy-start.3 = (f32[16]{0:T(128)S(1)}, f32[16]{0:T(128)}, u32[]{:S(2)}) copy-start(f32[16]{0:T(128)} %param.15) | copy-start | bytes 196
  49.9 21.5 %copy-start.4 = (f32[16]{0:T(128)S(1)}, f32[16]{0:T(128)}, u32[]{:S(2)}) copy-start(f32[16]{0:T(128)} %param.16) | copy-start | bytes 196
  54.5 12.3 %all-to-all-start.4 = ((bf16[4,128,512]{1,2,0:T(8,128)(2,1)}), bf16[4,128,512]{1,2,0:T(8,128)(2,1)S(1)}, u32[]{:S(2)}, u32[]{:S(2)}) async-start(bf16[4,128,512]{1,2,0:T(8,128)(2,1)} %copy.23), calls=%async_computation.4 | async-start | bytes 1048576 | tf_op jit(solution)/shard_map/all_to_all | solution.py:54
  66.8 10.6 %all-to-all-start.3 = ((bf16[128,4,1,128]{3,0,2,1:T(8,128)(2,1)}), bf16[128,4,1,128]{3,0,2,1:T(8,128)(2,1)S(1)}, u32[]{:S(2)}, u32[]{:S(2)}) async-start(bf16[128,4,1,128]{3,0,2,1:T(8,128)(2,1)} %bitcast.12), calls=%async_computation.3 | async-start | bytes 262144 | tf_op jit(solution)/shard_map/all_to_all | solution.py:83
  77.3 16.5 %all-to-all-start.5 = ((bf16[128,4,4,128]{3,0,2,1:T(8,128)(2,1)}), bf16[128,4,4,128]{3,0,2,1:T(8,128)(2,1)S(1)}, u32[]{:S(2)}, u32[]{:S(2)}) async-start(bf16[128,4,4,128]{3,0,2,1:T(8,128)(2,1)} %copy.24), calls=%async_computation.5 | async-start | bytes 1048576 | tf_op jit(solution)/shard_map/all_to_all | solution.py:81
  93.9 9.2 %all-to-all-start.1 = ((bf16[128,4,1,128]{3,0,2,1:T(8,128)(2,1)}), bf16[128,4,1,128]{3,0,2,1:T(8,128)(2,1)S(1)}, u32[]{:S(2)}, u32[]{:S(2)}) async-start(bf16[128,4,1,128]{3,0,2,1:T(8,128)(2,1)} %bitcast.4), calls=%async_computation.1 | async-start | bytes 262144 | tf_op jit(solution)/shard_map/all_to_all | solution.py:84
  99.2 1.9 %copy-start.1 = (f32[512,512,4]{1,0,2:T(8,128)}, f32[512,512,4]{1,0,2:T(8,128)S(1)}, u32[]{:S(2)}) copy-start(f32[512,512,4]{1,0,2:T(8,128)S(1)} %get-tuple-element.24) | copy-start | bytes 12582916
Sparse Core Ops, SparseCore 0:
  8.9 25.2 all-gather.1
where the time goes:
time: 134 us; the launch traced here: 133 us
  waiting for transfers between devices  46.2 us (34%)
  starting transfers between devices  29.1 us (22%)
  blocking collectives  17.5 us (13%)
  matrix products  15.8 us (12%)
  between operations  13.6 us (10%)
  local copies, waits for them, and re-layouts  6.66 us (5%)
  other arithmetic  4.19 us (3%)
    all_gather x1, waiting for transfers between devices, local(): everyone = lax.all_gather(tokens, 'dp', axis=0, tiled=True)  18.6 us
    all_to_all x1, blocking collectives, local(): lax.all_to_all(outputs, 'sp', split_axis=0, concat_axis=1, tiled=True)  17.5 us
    all_to_all x1, waiting for transfers between devices, local(): lax.all_to_all(query_send, 'sp', split_axis=1, concat_axis=0, tiled=True)  11.1 us
    all_to_all x1, waiting for transfers between devices, local(): lax.all_to_all(query_cols, 'dp', split_axis=0, concat_axis=2, tiled=True)  7.92 us
    all_to_all x1, starting transfers between devices, local(): lax.all_to_all(forget_send, 'sp', split_axis=1, concat_axis=0, tiled=True)  6.35 us
    all_to_all x1, waiting for transfers between devices, local(): lax.all_to_all(key_send, 'sp', split_axis=1, concat_axis=0, tiled=True)  4.79 us
    all_to_all x1, starting transfers between devices, local(): lax.all_to_all(key_send, 'sp', split_axis=1, concat_axis=0, tiled=True)  4.6 us
    all_to_all x1, starting transfers between devices, local(): lax.all_to_all(value_cols, 'dp', split_axis=0, concat_axis=2, tiled=True)  3.97 us
  transfers between devices with their start and end apart: 8, of which 7 were waited for; matrix products, arithmetic and copies ran while one was open for 14% of the time, Pallas kernels for 0%

commit v1 on v0

--- a/solution.py
+++ b/solution.py
@@ -1,6 +1,8 @@
 import jax
 import jax.numpy as jnp
 from jax import lax
+from jax.experimental import pallas as pl
+from jax.experimental.pallas import tpu as pltpu
 from jax.sharding import PartitionSpec as P
 
 NEG = -1e30
@@ -12,7 +14,7 @@
     return vectors * lax.rsqrt(jnp.mean(vectors * vectors, axis=-1, keepdims=True) + floor)
 
 
-def local(
+def heads_on_sp(
     tokens,
     forget_offset,
     q_weight,
@@ -133,6 +135,473 @@
     return back_rows.reshape(1, tok_count, head_count * head_dim)
 
 
+def heads_on_dp(
+    tokens,
+    forget_offset,
+    q_weight,
+    k_weight,
+    v_weight,
+    forget_weight,
+    forget_bias,
+    score_gain,
+    out_gain,
+):
+    tok_count = tokens.shape[1]
+    head_count = forget_bias.shape[0]
+    head_dim = out_gain.shape[0] // head_count
+    seq_count = lax.axis_size("dp")
+    kv = k_weight.shape[1] // head_dim
+    heads = q_weight.shape[1] // head_dim
+    group = heads // kv
+    everyone = lax.all_gather(tokens, "dp", axis=0, tiled=True)
+    offsets = lax.all_gather(forget_offset, "dp", axis=0, tiled=True)
+    flat = everyone.reshape(seq_count * tok_count, -1)
+    first = lax.axis_index("dp") * heads
+
+    def mine(array):
+        return lax.dynamic_slice_in_dim(array, first, heads, array.ndim - 1)
+
+    def project(weight):
+        return jnp.dot(flat, weight, preferred_element_type=jnp.float32).astype(jnp.bfloat16)
+
+    key_unit = head_norm(
+        project(k_weight).astype(jnp.float32).reshape(seq_count, tok_count, kv, head_dim), QK_FLOOR
+    ).astype(jnp.bfloat16)
+    values = project(v_weight).reshape(seq_count, tok_count, kv, head_dim)
+    pair = lax.all_gather(jnp.stack([key_unit, values]), "sp", axis=2, tiled=True)
+    forget_input = (
+        jnp.dot(flat, mine(forget_weight), preferred_element_type=jnp.float32)
+        + offsets.reshape(-1)[:, None]
+    ).astype(jnp.bfloat16)
+    log_gate = jax.nn.log_sigmoid(forget_input.astype(jnp.float32) + mine(forget_bias)[None, :])
+    gates = lax.all_gather(
+        log_gate.reshape(seq_count, tok_count, heads), "sp", axis=1, tiled=True
+    )
+    cumulative = jnp.cumsum(gates, axis=1)
+    length = gates.shape[1]
+    start = lax.axis_index("sp") * tok_count
+    own = lax.dynamic_slice_in_dim(cumulative, start, tok_count, 1)
+    query_unit = head_norm(
+        project(q_weight).astype(jnp.float32).reshape(seq_count, tok_count, kv, group, head_dim),
+        QK_FLOOR,
+    ).astype(jnp.bfloat16)
+    factor = (mine(score_gain) * head_dim ** (-0.5)).reshape(kv, group)
+    scores = jnp.einsum(
+        "bqkgd,bskd->bkgqs", query_unit, pair[0], preferred_element_type=jnp.float32
+    )
+    by_head = jnp.transpose(own.reshape(seq_count, tok_count, kv, group), (0, 2, 3, 1))
+    by_key = jnp.transpose(cumulative.reshape(seq_count, length, kv, group), (0, 2, 3, 1))
+    scores = (
+        scores * factor[None, :, :, None, None] + by_head[..., None] - by_key[..., None, :]
+    )
+    allowed = jnp.arange(length)[None, :] <= (start + jnp.arange(tok_count))[:, None]
+    scores = jnp.where(allowed, scores, NEG)
+    exponent = jnp.exp(scores - jnp.max(scores, axis=-1, keepdims=True))
+    weights = (exponent / jnp.sum(exponent, axis=-1, keepdims=True)).astype(jnp.bfloat16)
+    mixed = jnp.einsum(
+        "bkgqs,bskd->bqkgd", weights, pair[1], preferred_element_type=jnp.float32
+    )
+    gains = lax.dynamic_slice_in_dim(out_gain, first * head_dim, heads * head_dim, 0)
+    outputs = (head_norm(mixed, OUT_FLOOR) * gains.reshape(kv, group, head_dim)).astype(
+        jnp.bfloat16
+    )
+    outputs = outputs.reshape(seq_count, tok_count, heads * head_dim)
+    return lax.all_to_all(outputs, "dp", split_axis=0, concat_axis=2, tiled=True)
+
+
+def fused_kernel(
+    tok_in,
+    off_in,
+    qw_in,
+    kw_in,
+    vw_in,
+    fw_in,
+    bias_in,
+    gain_in,
+    norm_in,
+    out_ref,
+    tok,
+    qw,
+    kvw,
+    q_unit,
+    kv,
+    gate_send,
+    gates,
+    sent,
+    result,
+    load_sem,
+    tok_send,
+    tok_recv,
+    gate_send_sem,
+    gate_recv_sem,
+    kv_send_sem,
+    kv_recv_sem,
+    chain_send_sem,
+    chain_recv_sem,
+    out_send_sem,
+    out_recv_sem,
+    store_sem,
+):
+    d = lax.axis_index("dp")
+    s = lax.axis_index("sp")
+    spread = lax.axis_size("sp")
+    rows, width = tok_in.shape
+    half = rows // 2
+    cols = qw_in.shape[1]
+    head_dim = kw_in.shape[1]
+    heads = cols // head_dim
+    seqs = tok.shape[0]
+    chip, core = d // 2, d % 2
+    last = s == spread - 1
+
+    def peer(step):
+        return ((chip + step // 2) % 2) * 2 + (core + step % 2) % 2
+
+    def remote(src, dst, send, recv, **target):
+        return pltpu.make_async_remote_copy(
+            src_ref=src,
+            dst_ref=dst,
+            send_sem=send,
+            recv_sem=recv,
+            device_id=target,
+            device_id_type=pl.DeviceIdType.MESH,
+        )
+
+    load_tok = pltpu.make_async_copy(tok_in, tok.at[0], load_sem.at[0])
+    load_k = pltpu.make_async_copy(kw_in, kvw.at[:, pl.ds(0, head_dim)], load_sem.at[1])
+    load_v = pltpu.make_async_copy(vw_in, kvw.at[:, pl.ds(head_dim, head_dim)], load_sem.at[2])
+    load_q = pltpu.make_async_copy(qw_in, qw, load_sem.at[3])
+    load_tok.start()
+    load_k.start()
+    load_v.start()
+    load_q.start()
+
+    barrier = pltpu.get_barrier_semaphore()
+    for step in range(1, seqs):
+        pl.semaphore_signal(
+            barrier, inc=1, device_id={"dp": peer(step)}, device_id_type=pl.DeviceIdType.MESH
+        )
+
+    @pl.when(s > 0)
+    def _():
+        pl.semaphore_signal(
+            barrier, inc=1, device_id={"sp": s - 1}, device_id_type=pl.DeviceIdType.MESH
+        )
+
+    @pl.when(s < spread - 1)
+    def _():
+        pl.semaphore_signal(
+            barrier, inc=1, device_id={"sp": s + 1}, device_id_type=pl.DeviceIdType.MESH
+        )
+
+    pl.semaphore_wait(barrier, seqs - 1 + (s + spread - 1) // spread + 1 - (s + 1) // spread)
+
+    load_tok.wait()
+    parts = [pl.ds(0, half), pl.ds(half, half)]
+    over = [
+        remote(tok.at[0, part], tok.at[2, part], tok_send.at[1 + i], tok_recv.at[1 + i], dp=peer(2))
+        for i, part in enumerate(parts)
+    ]
+    beside = remote(tok.at[0], tok.at[1], tok_send.at[0], tok_recv.at[0], dp=peer(1))
+    onward = [
+        remote(tok.at[2, part], tok.at[3, part], tok_send.at[3 + i], tok_recv.at[3 + i], dp=peer(1))
+        for i, part in enumerate(parts)
+    ]
+    over[0].start()
+    beside.start()
+    over[1].start()
+
+    def unit(vectors):
+        vectors = vectors.astype(jnp.bfloat16).astype(jnp.float32)
+        return head_norm(vectors, QK_FLOOR).astype(jnp.bfloat16)
+
+    here = pl.ds(pl.multiple_of(s * rows, rows), rows)
+
+    def kv_copy(slot, block):
+        piece = kv.at[slot, :, pl.ds(pl.multiple_of(block * rows, rows), rows)]
+        return remote(
+            piece, piece, kv_send_sem.at[slot, block], kv_recv_sem.at[slot, block],
+            sp=(s + 1) % spread,
+        )
+
+    def gate_chain(block):
+        piece = gates.at[block]
+        return remote(
+            piece, piece, chain_send_sem.at[block], chain_recv_sem.at[block], sp=(s + 1) % spread
+        )
+
+    def project_kv(slot):
+        pair = jnp.dot(tok[slot], kvw[...], preferred_element_type=jnp.float32)
+        kv[slot, 0, here] = unit(pair[:, :head_dim])
+        kv[slot, 1, here] = pair[:, head_dim:].astype(jnp.bfloat16)
+
+        @pl.when(s < spread - 1)
+        def _():
+            kv_copy(slot, s).start()
+
+    def project_q(slot):
+        queries = jnp.dot(tok[slot], qw[...], preferred_element_type=jnp.float32)
+        for h in range(heads):
+            q_unit[slot, pl.ds(h * rows, rows)] = unit(
+                queries[:, h * head_dim : (h + 1) * head_dim]
+            )
+
+    load_k.wait()
+    load_v.wait()
+    project_kv(0)
+
+    forget_input = (
+        lax.dot_general(
+            fw_in[...], tok[0], (((1,), (1,)), ((), ())), preferred_element_type=jnp.float32
+        )
+        + off_in[...]
+    ).astype(jnp.bfloat16)
+    gate_arg = forget_input.astype(jnp.float32) + bias_in[...]
+    log_gate = jnp.minimum(gate_arg, 0.0) - jnp.log1p(jnp.exp(-jnp.abs(gate_arg)))
+    before = lax.broadcasted_iota(jnp.int32, (rows, rows), 0)
+    after = lax.broadcasted_iota(jnp.int32, (rows, rows), 1)
+    running = jnp.dot(
+        log_gate,
+        (before <= after).astype(jnp.float32),
+        preferred_element_type=jnp.float32,
+        precision=lax.Precision.HIGHEST,
+    )
+    gate_send[...] = jnp.zeros_like(gate_send)
+    for c in range(seqs):
+        gate_send[c, :heads, :] = running[c * heads : (c + 1) * heads]
+    gates[s, 0] = gate_send[d]
+    gate_out = [
+        remote(
+            gate_send.at[peer(step)], gates.at[s, step], gate_send_sem.at[step],
+            gate_recv_sem.at[step], dp=peer(step),
+        )
+        for step in range(1, seqs)
+    ]
+    for copy in gate_out:
+        copy.start()
+
+    beside.wait_recv()
+    project_kv(1)
+    load_q.wait()
+    project_q(0)
+    project_q(1)
+    for copy in gate_out:
+        copy.wait_recv()
+
+    @pl.when(s < spread - 1)
+    def _():
+        gate_chain(s).start()
+
+    def relay(k, slots, with_gates):
+        block = s - k
+        if with_gates:
+            gate_chain(block).wait_recv()
+
+            @pl.when(s < spread - 1)
+            def _():
+                gate_chain(block).start()
+
+        for slot in slots:
+            kv_copy(slot, block).wait_recv()
+
+            @pl.when(s < spread - 1)
+            def _():
+                kv_copy(slot, block).start()
+
+    def early(k, carry):
+        relay(k, (0, 1), True)
+        return carry
+
+    def late(k, carry):
+        relay(k, (2, 3), False)
+        return carry
+
+    lax.fori_loop(1, s + 1, early, 0)
+
+    for i in range(2):
+        over[i].wait_recv()
+        onward[i].start()
+    project_kv(2)
+    for i in range(2):
+        onward[i].wait_recv()
+    project_kv(3)
+    project_q(2)
+    project_q(3)
+
+    @pl.when(s < spread - 1)
+    def _():
+        lax.fori_loop(1, s + 1, late, 0)
+
+    mine = pl.ds(pl.multiple_of(d * cols, cols), cols)
+
+    def out_copy(slot):
+        return remote(
+            sent.at[slot], result.at[:, mine], out_send_sem.at[slot], out_recv_sem.at[slot],
+            dp=peer(slot),
+        )
+
+    def attend(slot, blocks):
+        span = blocks * rows
+        prefix = jnp.zeros((gates.shape[2], 1), jnp.float32)
+        totals = []
+        for b in range(blocks):
+            local_sum = gates[b, slot]
+            totals.append(local_sum + prefix)
+            prefix = prefix + local_sum[:, rows - 1 :]
+        by_row = jnp.transpose(totals[-1])
+        by_key = jnp.concatenate(totals, axis=1)
+        row = lax.broadcasted_iota(jnp.int32, (rows, span), 0) + (span - rows)
+        column = lax.broadcasted_iota(jnp.int32, (rows, span), 1)
+        allowed = column <= row
+        keys = kv[slot, 0, :span]
+        values = kv[slot, 1, :span]
+        for h in range(heads):
+            scores = lax.dot_general(
+                q_unit[slot, pl.ds(h * rows, rows)],
+                keys,
+                (((1,), (1,)), ((), ())),
+                preferred_element_type=jnp.float32,
+            )
+            factor = gain_in[0, d * heads + h] * head_dim ** (-0.5)
+            scores = scores * factor + by_row[:, h : h + 1] - by_key[h : h + 1, :]
+            scores = jnp.where(allowed, scores, NEG)
+            exponent = jnp.exp(scores - jnp.max(scores, axis=-1, keepdims=True))
+            scale = 1.0 / jnp.sum(exponent, axis=-1, keepdims=True)
+            weights = (exponent * scale).astype(jnp.bfloat16)
+            mixed = jnp.dot(weights, values, preferred_element_type=jnp.float32)
+            gain = norm_in[:, pl.ds(pl.multiple_of(d * cols + h * head_dim, head_dim), head_dim)]
+            sent[slot, :, h * head_dim : (h + 1) * head_dim] = (
+                head_norm(mixed, OUT_FLOOR) * gain
+            ).astype(jnp.bfloat16)
+
+    def each(slot, carry):
+        @pl.when(jnp.logical_and(last, slot >= 2))
+        def _():
+            def arrive(k, inner):
+                kv_copy(slot, s - k).wait_recv()
+                return inner
+
+            lax.fori_loop(1, s + 1, arrive, 0)
+
+        for k in range(spread):
+
+            @pl.when(s == k)
+            def _():
+                attend(slot, k + 1)
+
+        @pl.when(slot > 0)
+        def _():
+            out_copy(slot).start()
+
+        @pl.when(slot == 0)
+        def _():
+            result[:, mine] = sent[0]
+
+        return carry
+
+    lax.fori_loop(0, seqs, each, 0)
+
+    def flush(slot, carry):
+        out_copy(slot).wait_recv()
+        return carry
+
+    lax.fori_loop(1, seqs, flush, 0)
+    store = pltpu.make_async_copy(result, out_ref, store_sem.at[0])
+    store.start()
+    for slot in range(1, seqs):
+        out_copy(slot).wait_send()
+    for copy in over + [beside] + onward + gate_out:
+        copy.wait_send()
+
+    @pl.when(s < spread - 1)
+    def _():
+        def drain(block, carry):
+            gate_chain(block).wait_send()
+            for slot in range(seqs):
+                kv_copy(slot, block).wait_send()
+            return carry
+
+        lax.fori_loop(0, s + 1, drain, 0)
+
+    store.wait()
+
+
+def fused(
+    tokens,
+    forget_offset,
+    q_weight,
+    k_weight,
+    v_weight,
+    forget_weight,
+    forget_bias,
+    score_gain,
+    out_gain,
+):
+    rows, width = tokens.shape[1:]
+    head_count = forget_bias.shape[0]
+    head_dim = out_gain.shape[0] // head_count
+    seqs = lax.axis_size("dp")
+    spread = lax.axis_size("sp")
+    cols = q_weight.shape[1]
+    heads = cols // head_dim
+    padded = -(-heads // 8) * 8
+    anywhere = pl.BlockSpec(memory_space=pl.ANY)
+    vmem = pl.BlockSpec(memory_space=pltpu.VMEM)
+    dma = pltpu.SemaphoreType.DMA
+    out = pl.pallas_call(
+        fused_kernel,
+        out_shape=jax.ShapeDtypeStruct((rows, seqs * cols), jnp.bfloat16),
+        in_specs=[anywhere, vmem, anywhere, anywhere, anywhere, vmem, vmem,
+                  pl.BlockSpec(memory_space=pltpu.SMEM), vmem],
+        out_specs=anywhere,
+        scratch_shapes=[
+            pltpu.VMEM((seqs, rows, width), jnp.bfloat16),
+            pltpu.VMEM((width, cols), jnp.bfloat16),
+            pltpu.VMEM((width, 2 * head_dim), jnp.bfloat16),
+            pltpu.VMEM((seqs, heads * rows, head_dim), jnp.bfloat16),
+            pltpu.VMEM((seqs, 2, spread * rows, head_dim), jnp.bfloat16),
+            pltpu.VMEM((seqs, padded, rows), jnp.float32),
+            pltpu.VMEM((spread, seqs, padded, rows), jnp.float32),
+            pltpu.VMEM((seqs, rows, cols), jnp.bfloat16),
+            pltpu.VMEM((rows, seqs * cols), jnp.bfloat16),
+            dma((4,)),
+            dma((5,)),
+            dma((5,)),
+            dma((seqs,)),
+            dma((seqs,)),
+            dma((seqs, spread)),
+            dma((seqs, spread)),
+            dma((spread,)),
+            dma((spread,)),
+            dma((seqs,)),
+            dma((seqs,)),
+            dma((1,)),
+        ],
+        compiler_params=pltpu.CompilerParams(collective_id=0, has_side_effects=True),
+    )(
+        tokens[0],
+        forget_offset,
+        q_weight,
+        k_weight,
+        v_weight,
+        forget_weight.T,
+        forget_bias[:, None],
+        score_gain[None, :],
+        out_gain[None, :],
+    )
+    return out[None]
+
+
+def local(*args):
+    tokens, k_weight, forget_bias, out_gain = args[0], args[3], args[6], args[8]
+    head_dim = out_gain.shape[0] // forget_bias.shape[0]
+    if lax.axis_size("dp") == 4 and k_weight.shape[1] == head_dim and tokens.shape[0] == 1:
+        return fused(*args)
+    if k_weight.shape[1] % head_dim == 0 and tokens.shape[0] == 1:
+        return heads_on_dp(*args)
+    return heads_on_sp(*args)
+
+
 def solution(mesh):
     in_specs = (
         P(("grp", "dp"), "sp", None),

time: 134 us -> 46.3 us (0.35)
  the two profiles are of different devices: /device:TPU:0 before, /device:TPU:25 now
where the time goes in v1:
time: 46.3 us; the launch traced here: 46.1 us
  Pallas kernels  42.9 us (93%)
  local copies, waits for them, and re-layouts  3.21 us (7%)
    pallas_call x1, Pallas kernels, fused(): pl.pallas_call(fused_kernel, out_shape=jax.ShapeDtypeStruct((rows, seqs *...  42.9 us
    unnamed x1, local copies, waits for them, and re-layouts  1.88 us
    broadcast_in_dim x1, local copies, waits for them, and re-layouts, fused(): forget_bias[:, None]  1.33 us

profile of v1, /device:TPU:25, one launch (start us, length us, event | category | flops | bytes accessed | tf_op | source)
XLA Modules:
  0.0 46.1 jit_solution(6459809107748692670)
XLA Ops:
  0.0 1.3 %copy.10.bias_in = f32[16,1]{1,0:T(8,128)} copy(f32[16,1]{0,1:T(1,128)} %bitcast.11) | data formatting | bytes 128 | tf_op jit(solution)/shard_map/broadcast_in_dim | solution.py:588
  1.3 42.9 %shard_map.91 = bf16[128,2048]{1,0:T(8,128)(2,1)} custom-call(bf16[128,2048]{1,0:T(8,128)(2,1)} %bitcast.7, f32[1,128]{1,0:T(1,128)} %off_in.1, bf16[2048,512]{1,0:T(8,128)(2,1)} %qw_in.1, bf16[2048,128]{1,0:T(8,128)(2,1)} %kw_in.1, bf16[2048,128]{1,0:T(8,128)(2,1)} %vw_in.1, bf16[16,2048]{1,0:T(8,128)(2,1)} %bitcast.8, f32[16,1]{1,0:T(8,128)} %copy.10.bias_in, ...), custom_call_target="tpu_custom_call" | custom-call | tf_op jit(solution)/shard_map/pallas_call | solution.py:551
  44.2 1.9 %copy.12 = bf16[1,128,2048]{2,1,0:T(8,128)(2,1)} copy(bf16[1,128,2048]{2,1,0:T(8,128)(2,1)} %bitcast.6) | data formatting | bytes 1048576

commit v2 on v1

--- a/solution.py
+++ b/solution.py
@@ -317,10 +317,17 @@
 
     here = pl.ds(pl.multiple_of(s * rows, rows), rows)
 
-    def kv_copy(slot, block):
-        piece = kv.at[slot, :, pl.ds(pl.multiple_of(block * rows, rows), rows)]
+    def pieces(slot):
+        return 1 if slot < 2 else 2
+
+    def stretch(slot, piece, block):
+        size = rows // pieces(slot)
+        return pl.ds(pl.multiple_of(block * rows + piece * size, size), size)
+
+    def kv_copy(slot, piece, block):
+        part = kv.at[slot, :, stretch(slot, piece, block)]
         return remote(
-            piece, piece, kv_send_sem.at[slot, block], kv_recv_sem.at[slot, block],
+            part, part, kv_send_sem.at[slot, piece, block], kv_recv_sem.at[slot, piece, block],
             sp=(s + 1) % spread,
         )
 
@@ -330,14 +337,19 @@
             piece, piece, chain_send_sem.at[block], chain_recv_sem.at[block], sp=(s + 1) % spread
         )
 
-    def project_kv(slot):
-        pair = jnp.dot(tok[slot], kvw[...], preferred_element_type=jnp.float32)
-        kv[slot, 0, here] = unit(pair[:, :head_dim])
-        kv[slot, 1, here] = pair[:, head_dim:].astype(jnp.bfloat16)
+    def project_kv(slot, piece):
+        size = rows // pieces(slot)
+        pair = jnp.dot(
+            tok[slot, piece * size : (piece + 1) * size], kvw[...],
+            preferred_element_type=jnp.float32,
+        )
+        place = stretch(slot, piece, s)
+        kv[slot, 0, place] = unit(pair[:, :head_dim])
+        kv[slot, 1, place] = pair[:, head_dim:].astype(jnp.bfloat16)
 
         @pl.when(s < spread - 1)
         def _():
-            kv_copy(slot, s).start()
+            kv_copy(slot, piece, s).start()
 
     def project_q(slot):
         queries = jnp.dot(tok[slot], qw[...], preferred_element_type=jnp.float32)
@@ -348,7 +360,7 @@
 
     load_k.wait()
     load_v.wait()
-    project_kv(0)
+    project_kv(0, 0)
 
     forget_input = (
         lax.dot_general(
@@ -356,7 +368,15 @@
         )
         + off_in[...]
     ).astype(jnp.bfloat16)
-    gate_arg = forget_input.astype(jnp.float32) + bias_in[...]
+    count = bias_in.shape[1]
+    square = (count, count)
+    diagonal = lax.broadcasted_iota(jnp.int32, square, 0) == lax.broadcasted_iota(
+        jnp.int32, square, 1
+    )
+    bias = jnp.sum(
+        jnp.where(diagonal, jnp.broadcast_to(bias_in[...], square), 0.0), axis=1, keepdims=True
+    )
+    gate_arg = forget_input.astype(jnp.float32) + bias
     log_gate = jnp.minimum(gate_arg, 0.0) - jnp.log1p(jnp.exp(-jnp.abs(gate_arg)))
     before = lax.broadcasted_iota(jnp.int32, (rows, rows), 0)
     after = lax.broadcasted_iota(jnp.int32, (rows, rows), 1)
@@ -381,10 +401,30 @@
         copy.start()
 
     beside.wait_recv()
-    project_kv(1)
+    project_kv(1, 0)
     load_q.wait()
     project_q(0)
-    project_q(1)
+
+    def relay(first, stop, units, with_gates=False):
+        @pl.when(s < spread - 1)
+        def _():
+            def one(k, carry):
+                block = s - k
+                if with_gates:
+                    gate_chain(block).wait_recv()
+                    gate_chain(block).start()
+                for slot, piece in units:
+                    kv_copy(slot, piece, block).wait_recv()
+                    kv_copy(slot, piece, block).start()
+                return carry
+
+            lax.fori_loop(first, stop, one, 0)
+
+    some = (s + spread - 1) // spread
+    relay(1, 1 + some, [(0, 0), (1, 0)])
+    over[0].wait_recv()
+    onward[0].start()
+    project_kv(2, 0)
     for copy in gate_out:
         copy.wait_recv()
 
@@ -392,45 +432,20 @@
     def _():
         gate_chain(s).start()
 
-    def relay(k, slots, with_gates):
-        block = s - k
-        if with_gates:
-            gate_chain(block).wait_recv()
-
-            @pl.when(s < spread - 1)
-            def _():
-                gate_chain(block).start()
-
-        for slot in slots:
-            kv_copy(slot, block).wait_recv()
-
-            @pl.when(s < spread - 1)
-            def _():
-                kv_copy(slot, block).start()
-
-    def early(k, carry):
-        relay(k, (0, 1), True)
-        return carry
-
-    def late(k, carry):
-        relay(k, (2, 3), False)
-        return carry
-
-    lax.fori_loop(1, s + 1, early, 0)
-
-    for i in range(2):
-        over[i].wait_recv()
-        onward[i].start()
-    project_kv(2)
-    for i in range(2):
-        onward[i].wait_recv()
-    project_kv(3)
+    project_q(1)
+    onward[0].wait_recv()
+    project_kv(3, 0)
+    relay(2, s + 1, [(0, 0), (1, 0)])
+    relay(1, s + 1, [(2, 0), (3, 0)], True)
+    over[1].wait_recv()
+    onward[1].start()
+    project_kv(2, 1)
+    onward[1].wait_recv()
+    project_kv(3, 1)
     project_q(2)
+    relay(1, 1 + some, [(2, 1), (3, 1)])
     project_q(3)
-
-    @pl.when(s < spread - 1)
-    def _():
-        lax.fori_loop(1, s + 1, late, 0)
+    relay(2, s + 1, [(2, 1), (3, 1)])
 
     mine = pl.ds(pl.multiple_of(d * cols, cols), cols)
 
@@ -475,13 +490,18 @@
             ).astype(jnp.bfloat16)
 
     def each(slot, carry):
-        @pl.when(jnp.logical_and(last, slot >= 2))
-        def _():
-            def arrive(k, inner):
-                kv_copy(slot, s - k).wait_recv()
-                return inner
-
-            lax.fori_loop(1, s + 1, arrive, 0)
+        for known in range(seqs):
+
+            @pl.when(jnp.logical_and(last, slot == known))
+            def _():
+                def arrive(k, inner):
+                    if known == 0:
+                        gate_chain(s - k).wait_recv()
+                    for piece in range(pieces(known)):
+                        kv_copy(known, piece, s - k).wait_recv()
+                    return inner
+
+                lax.fori_loop(1, s + 1, arrive, 0)
 
         for k in range(spread):
 
@@ -518,7 +538,8 @@
         def drain(block, carry):
             gate_chain(block).wait_send()
             for slot in range(seqs):
-                kv_copy(slot, block).wait_send()
+                for piece in range(pieces(slot)):
+                    kv_copy(slot, piece, block).wait_send()
             return carry
 
         lax.fori_loop(0, s + 1, drain, 0)
@@ -569,8 +590,8 @@
             dma((5,)),
             dma((seqs,)),
             dma((seqs,)),
-            dma((seqs, spread)),
-            dma((seqs, spread)),
+            dma((seqs, 2, spread)),
+            dma((seqs, 2, spread)),
             dma((spread,)),
             dma((spread,)),
             dma((seqs,)),
@@ -585,7 +606,7 @@
         k_weight,
         v_weight,
         forget_weight.T,
-        forget_bias[:, None],
+        forget_bias[None, :],
         score_gain[None, :],
         out_gain[None, :],
     )

time: 46.3 us -> 42 us (0.907); the launches traced: 46.1 us -> 41.3 us
  Pallas kernels: 42.9 us -> 39.4 us
  local copies, waits for them, and re-layouts: 3.21 us -> 1.88 us
    pallas_call x1, Pallas kernels: 42.9 us -> 39.4 us  [fused(): pl.pallas_call(fused_kernel, out_shape=jax.ShapeDtypeStruct((rows, seqs *...]
    broadcast_in_dim x1 -> x0, local copies, waits for them, and re-layouts: 1.33 us -> none  [fused(): forget_bias[:, None]]
where the time goes in v2:
time: 42 us; the launch traced here: 41.3 us
  Pallas kernels  39.4 us (94%)
  local copies, waits for them, and re-layouts  1.88 us (4%)
    pallas_call x1, Pallas kernels, fused(): pl.pallas_call(fused_kernel, out_shape=jax.ShapeDtypeStruct((rows, seqs *...  39.4 us
    unnamed x1, local copies, waits for them, and re-layouts  1.88 us

profile of v2, /device:TPU:25, one launch (start us, length us, event | category | flops | bytes accessed | tf_op | source)
XLA Modules:
  0.0 41.3 jit_solution(3858577444441529352)
XLA Ops:
  0.0 39.4 %shard_map.91 = bf16[128,2048]{1,0:T(8,128)(2,1)} custom-call(bf16[128,2048]{1,0:T(8,128)(2,1)} %bitcast.7, f32[1,128]{1,0:T(1,128)} %off_in.1, bf16[2048,512]{1,0:T(8,128)(2,1)} %qw_in.1, bf16[2048,128]{1,0:T(8,128)(2,1)} %kw_in.1, bf16[2048,128]{1,0:T(8,128)(2,1)} %vw_in.1, bf16[16,2048]{1,0:T(8,128)(2,1)} %bitcast.8, f32[1,16]{1,0:T(1,128)} %bitcast.10, ...), custom_call_target="tpu_custom_call" | custom-call | tf_op jit(solution)/shard_map/pallas_call | solution.py:572
  39.4 1.9 %copy.11 = bf16[1,128,2048]{2,1,0:T(8,128)(2,1)} copy(bf16[1,128,2048]{2,1,0:T(8,128)(2,1)} %bitcast.6) | data formatting | bytes 1048576

commit v3 on v2

--- a/solution.py
+++ b/solution.py
@@ -8,6 +8,7 @@
 NEG = -1e30
 QK_FLOOR = 0.1
 OUT_FLOOR = 0.001
+SPLITS = 2
 
 
 def head_norm(vectors, floor):
@@ -246,7 +247,8 @@
     s = lax.axis_index("sp")
     spread = lax.axis_size("sp")
     rows, width = tok_in.shape
-    half = rows // 2
+    splits = kv_send_sem.shape[1]
+    size = rows // splits
     cols = qw_in.shape[1]
     head_dim = kw_in.shape[1]
     heads = cols // head_dim
@@ -297,19 +299,20 @@
     pl.semaphore_wait(barrier, seqs - 1 + (s + spread - 1) // spread + 1 - (s + 1) // spread)
 
     load_tok.wait()
-    parts = [pl.ds(0, half), pl.ds(half, half)]
+    parts = [pl.ds(i * size, size) for i in range(splits)]
     over = [
         remote(tok.at[0, part], tok.at[2, part], tok_send.at[1 + i], tok_recv.at[1 + i], dp=peer(2))
         for i, part in enumerate(parts)
     ]
     beside = remote(tok.at[0], tok.at[1], tok_send.at[0], tok_recv.at[0], dp=peer(1))
     onward = [
-        remote(tok.at[2, part], tok.at[3, part], tok_send.at[3 + i], tok_recv.at[3 + i], dp=peer(1))
+        remote(tok.at[2, part], tok.at[3, part], tok_send.at[1 + splits + i], tok_recv.at[1 + splits + i], dp=peer(1))
         for i, part in enumerate(parts)
     ]
     over[0].start()
     beside.start()
-    over[1].start()
+    for copy in over[1:]:
+        copy.start()
 
     def unit(vectors):
         vectors = vectors.astype(jnp.bfloat16).astype(jnp.float32)
@@ -318,7 +321,7 @@
     here = pl.ds(pl.multiple_of(s * rows, rows), rows)
 
     def pieces(slot):
-        return 1 if slot < 2 else 2
+        return 1 if slot < 2 else splits
 
     def stretch(slot, piece, block):
         size = rows // pieces(slot)
@@ -419,33 +422,6 @@
                 return carry
 
             lax.fori_loop(first, stop, one, 0)
-
-    some = (s + spread - 1) // spread
-    relay(1, 1 + some, [(0, 0), (1, 0)])
-    over[0].wait_recv()
-    onward[0].start()
-    project_kv(2, 0)
-    for copy in gate_out:
-        copy.wait_recv()
-
-    @pl.when(s < spread - 1)
-    def _():
-        gate_chain(s).start()
-
-    project_q(1)
-    onward[0].wait_recv()
-    project_kv(3, 0)
-    relay(2, s + 1, [(0, 0), (1, 0)])
-    relay(1, s + 1, [(2, 0), (3, 0)], True)
-    over[1].wait_recv()
-    onward[1].start()
-    project_kv(2, 1)
-    onward[1].wait_recv()
-    project_kv(3, 1)
-    project_q(2)
-    relay(1, 1 + some, [(2, 1), (3, 1)])
-    project_q(3)
-    relay(2, s + 1, [(2, 1), (3, 1)])
 
     mine = pl.ds(pl.multiple_of(d * cols, cols), cols)
 
@@ -489,37 +465,72 @@
                 head_norm(mixed, OUT_FLOOR) * gain
             ).astype(jnp.bfloat16)
 
-    def each(slot, carry):
-        for known in range(seqs):
-
-            @pl.when(jnp.logical_and(last, slot == known))
+    def finish(first, stop, places):
+        def each(slot, carry):
+            for known in range(first, stop):
+                if spread - 1 in places:
+
+                    @pl.when(jnp.logical_and(last, slot == known))
+                    def _():
+                        def arrive(k, inner):
+                            if known == 0:
+                                gate_chain(s - k).wait_recv()
+                            for piece in range(pieces(known)):
+                                kv_copy(known, piece, s - k).wait_recv()
+                            return inner
+
+                        lax.fori_loop(1, s + 1, arrive, 0)
+
+            for k in places:
+
+                @pl.when(s == k)
+                def _():
+                    attend(slot, k + 1)
+
+                    @pl.when(slot > 0)
+                    def _():
+                        out_copy(slot).start()
+
+                    @pl.when(slot == 0)
+                    def _():
+                        result[:, mine] = sent[0]
+
+            return carry
+
+        lax.fori_loop(first, stop, each, 0)
+
+    some = (s + spread - 1) // spread
+    relay(1, 1 + some, [(0, 0), (1, 0)])
+    for i in range(splits):
+        over[i].wait_recv()
+        onward[i].start()
+        project_kv(2, i)
+        if i == 0:
+            for copy in gate_out:
+                copy.wait_recv()
+
+            @pl.when(s < spread - 1)
             def _():
-                def arrive(k, inner):
-                    if known == 0:
-                        gate_chain(s - k).wait_recv()
-                    for piece in range(pieces(known)):
-                        kv_copy(known, piece, s - k).wait_recv()
-                    return inner
-
-                lax.fori_loop(1, s + 1, arrive, 0)
-
-        for k in range(spread):
-
-            @pl.when(s == k)
-            def _():
-                attend(slot, k + 1)
-
-        @pl.when(slot > 0)
-        def _():
-            out_copy(slot).start()
-
-        @pl.when(slot == 0)
-        def _():
-            result[:, mine] = sent[0]
-
-        return carry
-
-    lax.fori_loop(0, seqs, each, 0)
+                gate_chain(s).start()
+
+            project_q(1)
+        onward[i].wait_recv()
+        project_kv(3, i)
+        if i == 0:
+            relay(2, s + 1, [(0, 0), (1, 0)])
+        if i < splits - 1:
+            relay(1, s + 1, [(2, i), (3, i)], i == 0)
+        if i == splits - 2:
+            finish(0, 2, [spread - 1])
+    others = list(range(spread - 1))
+    project_q(2)
+    relay(1, 1 + some, [(2, splits - 1), (3, splits - 1)])
+    project_q(3)
+    finish(0, 1, others)
+    relay(2, s + 1, [(2, splits - 1), (3, splits - 1)])
+    finish(1, 2, others)
+    finish(2, seqs, others + [spread - 1])
+
 
     def flush(slot, carry):
         out_copy(slot).wait_recv()
@@ -586,12 +597,12 @@
             pltpu.VMEM((seqs, rows, cols), jnp.bfloat16),
             pltpu.VMEM((rows, seqs * cols), jnp.bfloat16),
             dma((4,)),
-            dma((5,)),
-            dma((5,)),
+            dma((1 + 2 * SPLITS,)),
+            dma((1 + 2 * SPLITS,)),
             dma((seqs,)),
             dma((seqs,)),
-            dma((seqs, 2, spread)),
-            dma((seqs, 2, spread)),
+            dma((seqs, SPLITS, spread)),
+            dma((seqs, SPLITS, spread)),
             dma((spread,)),
             dma((spread,)),
             dma((seqs,)),

time: 42 us -> 44.2 us (1.052)
  Pallas kernels: 39.4 us -> 41.9 us
    pallas_call x1, Pallas kernels: 39.4 us -> 41.9 us  [fused(): pl.pallas_call(fused_kernel, out_shape=jax.ShapeDtypeStruct((rows, seqs *...]
where the time goes in v3:
time: 44.2 us; the launch traced here: 43.8 us
  Pallas kernels  41.9 us (95%)
  local copies, waits for them, and re-layouts  1.88 us (4%)
    pallas_call x1, Pallas kernels, fused(): pl.pallas_call(fused_kernel, out_shape=jax.ShapeDtypeStruct((rows, seqs *...  41.9 us
    unnamed x1, local copies, waits for them, and re-layouts  1.88 us

profile of v3, /device:TPU:25, one launch (start us, length us, event | category | flops | bytes accessed | tf_op | source)
XLA Modules:
  0.0 43.8 jit_solution(13571790929609335090)
XLA Ops:
  0.0 41.9 %shard_map.91 = bf16[128,2048]{1,0:T(8,128)(2,1)} custom-call(bf16[128,2048]{1,0:T(8,128)(2,1)} %bitcast.7, f32[1,128]{1,0:T(1,128)} %off_in.1, bf16[2048,512]{1,0:T(8,128)(2,1)} %qw_in.1, bf16[2048,128]{1,0:T(8,128)(2,1)} %kw_in.1, bf16[2048,128]{1,0:T(8,128)(2,1)} %vw_in.1, bf16[16,2048]{1,0:T(8,128)(2,1)} %bitcast.8, f32[1,16]{1,0:T(1,128)} %bitcast.10, ...), custom_call_target="tpu_custom_call" | custom-call | tf_op jit(solution)/shard_map/pallas_call | solution.py:583
  41.9 1.9 %copy.11 = bf16[1,128,2048]{2,1,0:T(8,128)(2,1)} copy(bf16[1,128,2048]{2,1,0:T(8,128)(2,1)} %bitcast.6) | data formatting | bytes 1048576

commit v4 on v3

--- a/solution.py
+++ b/solution.py
@@ -8,7 +8,6 @@
 NEG = -1e30
 QK_FLOOR = 0.1
 OUT_FLOOR = 0.001
-SPLITS = 2
 
 
 def head_norm(vectors, floor):
@@ -247,8 +246,7 @@
     s = lax.axis_index("sp")
     spread = lax.axis_size("sp")
     rows, width = tok_in.shape
-    splits = kv_send_sem.shape[1]
-    size = rows // splits
+    half = rows // 2
     cols = qw_in.shape[1]
     head_dim = kw_in.shape[1]
     heads = cols // head_dim
@@ -257,7 +255,12 @@
     last = s == spread - 1
 
     def peer(step):
-        return ((chip + step // 2) % 2) * 2 + (core + step % 2) % 2
+        across = step // 2
+        own_chip = (1 - across) * ((core + step % 2) % 2)
+        return ((chip + across) % 2) * 2 + across * (step % 2) + own_chip
+
+    def seen_as(step):
+        return (step // 2) * (2 + core) + (1 - step // 2) * step
 
     def remote(src, dst, send, recv, **target):
         return pltpu.make_async_remote_copy(
@@ -299,20 +302,27 @@
     pl.semaphore_wait(barrier, seqs - 1 + (s + spread - 1) // spread + 1 - (s + 1) // spread)
 
     load_tok.wait()
-    parts = [pl.ds(i * size, size) for i in range(splits)]
+    part = pl.ds(pl.multiple_of(core * half, half), half)
+    beside = remote(tok.at[0], tok.at[1], tok_send.at[0], tok_recv.at[0], dp=peer(1))
     over = [
-        remote(tok.at[0, part], tok.at[2, part], tok_send.at[1 + i], tok_recv.at[1 + i], dp=peer(2))
-        for i, part in enumerate(parts)
+        remote(
+            tok.at[held, part], tok.at[2 + i, part], tok_send.at[1 + i], tok_recv.at[1 + i],
+            dp=(1 - chip) * 2 + core,
+        )
+        for i, held in enumerate((core, 1 - core))
     ]
-    beside = remote(tok.at[0], tok.at[1], tok_send.at[0], tok_recv.at[0], dp=peer(1))
     onward = [
-        remote(tok.at[2, part], tok.at[3, part], tok_send.at[1 + splits + i], tok_recv.at[1 + splits + i], dp=peer(1))
-        for i, part in enumerate(parts)
+        remote(
+            tok.at[2 + i, part], tok.at[2 + i, part], tok_send.at[3 + i], tok_recv.at[3 + i],
+            dp=peer(1),
+        )
+        for i in range(2)
     ]
-    over[0].start()
     beside.start()
-    for copy in over[1:]:
-        copy.start()
+
+    @pl.when(core == 0)
+    def _():
+        over[0].start()
 
     def unit(vectors):
         vectors = vectors.astype(jnp.bfloat16).astype(jnp.float32)
@@ -320,17 +330,10 @@
 
     here = pl.ds(pl.multiple_of(s * rows, rows), rows)
 
-    def pieces(slot):
-        return 1 if slot < 2 else splits
-
-    def stretch(slot, piece, block):
-        size = rows // pieces(slot)
-        return pl.ds(pl.multiple_of(block * rows + piece * size, size), size)
-
-    def kv_copy(slot, piece, block):
-        part = kv.at[slot, :, stretch(slot, piece, block)]
+    def kv_copy(slot, block):
+        piece = kv.at[slot, :, pl.ds(pl.multiple_of(block * rows, rows), rows)]
         return remote(
-            part, part, kv_send_sem.at[slot, piece, block], kv_recv_sem.at[slot, piece, block],
+            piece, piece, kv_send_sem.at[slot, block], kv_recv_sem.at[slot, block],
             sp=(s + 1) % spread,
         )
 
@@ -340,19 +343,14 @@
             piece, piece, chain_send_sem.at[block], chain_recv_sem.at[block], sp=(s + 1) % spread
         )
 
-    def project_kv(slot, piece):
-        size = rows // pieces(slot)
-        pair = jnp.dot(
-            tok[slot, piece * size : (piece + 1) * size], kvw[...],
-            preferred_element_type=jnp.float32,
-        )
-        place = stretch(slot, piece, s)
-        kv[slot, 0, place] = unit(pair[:, :head_dim])
-        kv[slot, 1, place] = pair[:, head_dim:].astype(jnp.bfloat16)
+    def project_kv(slot):
+        pair = jnp.dot(tok[slot], kvw[...], preferred_element_type=jnp.float32)
+        kv[slot, 0, here] = unit(pair[:, :head_dim])
+        kv[slot, 1, here] = pair[:, head_dim:].astype(jnp.bfloat16)
 
         @pl.when(s < spread - 1)
         def _():
-            kv_copy(slot, piece, s).start()
+            kv_copy(slot, s).start()
 
     def project_q(slot):
         queries = jnp.dot(tok[slot], qw[...], preferred_element_type=jnp.float32)
@@ -363,7 +361,14 @@
 
     load_k.wait()
     load_v.wait()
-    project_kv(0, 0)
+    project_kv(0)
+    beside.wait_recv()
+
+    @pl.when(core == 1)
+    def _():
+        over[0].start()
+
+    over[1].start()
 
     forget_input = (
         lax.dot_general(
@@ -395,16 +400,15 @@
     gates[s, 0] = gate_send[d]
     gate_out = [
         remote(
-            gate_send.at[peer(step)], gates.at[s, step], gate_send_sem.at[step],
-            gate_recv_sem.at[step], dp=peer(step),
+            gate_send.at[peer(step)], gates.at[s, seen_as(step)], gate_send_sem.at[step],
+            gate_recv_sem.at[seen_as(step)], dp=peer(step),
         )
         for step in range(1, seqs)
     ]
     for copy in gate_out:
         copy.start()
 
-    beside.wait_recv()
-    project_kv(1, 0)
+    project_kv(1)
     load_q.wait()
     project_q(0)
 
@@ -416,18 +420,18 @@
                 if with_gates:
                     gate_chain(block).wait_recv()
                     gate_chain(block).start()
-                for slot, piece in units:
-                    kv_copy(slot, piece, block).wait_recv()
-                    kv_copy(slot, piece, block).start()
+                for slot in units:
+                    kv_copy(slot, block).wait_recv()
+                    kv_copy(slot, block).start()
                 return carry
 
             lax.fori_loop(first, stop, one, 0)
 
     mine = pl.ds(pl.multiple_of(d * cols, cols), cols)
 
-    def out_copy(slot):
+    def out_copy(slot, arrival):
         return remote(
-            sent.at[slot], result.at[:, mine], out_send_sem.at[slot], out_recv_sem.at[slot],
+            sent.at[slot], result.at[:, mine], out_send_sem.at[slot], out_recv_sem.at[arrival],
             dp=peer(slot),
         )
 
@@ -473,10 +477,9 @@
                     @pl.when(jnp.logical_and(last, slot == known))
                     def _():
                         def arrive(k, inner):
-                            if known == 0:
+                            if known == 2:
                                 gate_chain(s - k).wait_recv()
-                            for piece in range(pieces(known)):
-                                kv_copy(known, piece, s - k).wait_recv()
+                            kv_copy(known, s - k).wait_recv()
                             return inner
 
                         lax.fori_loop(1, s + 1, arrive, 0)
@@ -489,7 +492,7 @@
 
                     @pl.when(slot > 0)
                     def _():
-                        out_copy(slot).start()
+                        out_copy(slot, seen_as(slot)).start()
 
                     @pl.when(slot == 0)
                     def _():
@@ -500,47 +503,47 @@
         lax.fori_loop(first, stop, each, 0)
 
     some = (s + spread - 1) // spread
-    relay(1, 1 + some, [(0, 0), (1, 0)])
-    for i in range(splits):
-        over[i].wait_recv()
-        onward[i].start()
-        project_kv(2, i)
-        if i == 0:
-            for copy in gate_out:
-                copy.wait_recv()
-
-            @pl.when(s < spread - 1)
-            def _():
-                gate_chain(s).start()
-
-            project_q(1)
-        onward[i].wait_recv()
-        project_kv(3, i)
-        if i == 0:
-            relay(2, s + 1, [(0, 0), (1, 0)])
-        if i < splits - 1:
-            relay(1, s + 1, [(2, i), (3, i)], i == 0)
-        if i == splits - 2:
-            finish(0, 2, [spread - 1])
+    relay(1, 1 + some, [0, 1])
+    over[0].wait_recv()
+    onward[0].start()
+    for step in range(1, seqs):
+        pltpu.make_async_copy(
+            gates.at[s, step], gates.at[s, step], gate_recv_sem.at[step]
+        ).wait()
+
+    @pl.when(s < spread - 1)
+    def _():
+        gate_chain(s).start()
+
+    onward[0].wait_recv()
+    project_kv(2)
+    project_q(1)
+    relay(2, s + 1, [0, 1])
+    relay(1, s + 1, [2], True)
+    over[1].wait_recv()
+    onward[1].start()
+    project_q(2)
+    onward[1].wait_recv()
+    project_kv(3)
     others = list(range(spread - 1))
-    project_q(2)
-    relay(1, 1 + some, [(2, splits - 1), (3, splits - 1)])
+    everywhere = list(range(spread))
+    relay(1, 1 + some, [3])
+    finish(2, 3, everywhere)
     project_q(3)
-    finish(0, 1, others)
-    relay(2, s + 1, [(2, splits - 1), (3, splits - 1)])
-    finish(1, 2, others)
-    finish(2, seqs, others + [spread - 1])
-
+    relay(2, s + 1, [3])
+    finish(0, 2, [spread - 1])
+    finish(3, seqs, everywhere)
+    finish(0, 2, others)
 
     def flush(slot, carry):
-        out_copy(slot).wait_recv()
+        out_copy(slot, slot).wait_recv()
         return carry
 
     lax.fori_loop(1, seqs, flush, 0)
     store = pltpu.make_async_copy(result, out_ref, store_sem.at[0])
     store.start()
     for slot in range(1, seqs):
-        out_copy(slot).wait_send()
+        out_copy(slot, slot).wait_send()
     for copy in over + [beside] + onward + gate_out:
         copy.wait_send()
 
@@ -549,8 +552,7 @@
         def drain(block, carry):
             gate_chain(block).wait_send()
             for slot in range(seqs):
-                for piece in range(pieces(slot)):
-                    kv_copy(slot, piece, block).wait_send()
+                kv_copy(slot, block).wait_send()
             return carry
 
         lax.fori_loop(0, s + 1, drain, 0)
@@ -597,12 +599,12 @@
             pltpu.VMEM((seqs, rows, cols), jnp.bfloat16),
             pltpu.VMEM((rows, seqs * cols), jnp.bfloat16),
             dma((4,)),
-            dma((1 + 2 * SPLITS,)),
-            dma((1 + 2 * SPLITS,)),
+            dma((5,)),
+            dma((5,)),
             dma((seqs,)),
             dma((seqs,)),
-            dma((seqs, SPLITS, spread)),
-            dma((seqs, SPLITS, spread)),
+            dma((seqs, spread)),
+            dma((seqs, spread)),
             dma((spread,)),
             dma((spread,)),
             dma((seqs,)),

time: 44.2 us -> 41.9 us (0.948)
  Pallas kernels: 41.9 us -> 39.8 us
    pallas_call x1, Pallas kernels: 41.9 us -> 39.8 us  [fused(): pl.pallas_call(fused_kernel, out_shape=jax.ShapeDtypeStruct((rows, seqs *...]
where the time goes in v4:
time: 41.9 us; the launch traced here: 41.7 us
  Pallas kernels  39.8 us (95%)
  local copies, waits for them, and re-layouts  1.88 us (4%)
    pallas_call x1, Pallas kernels, fused(): pl.pallas_call(fused_kernel, out_shape=jax.ShapeDtypeStruct((rows, seqs *...  39.8 us
    unnamed x1, local copies, waits for them, and re-layouts  1.88 us

profile of v4, /device:TPU:25, one launch (start us, length us, event | category | flops | bytes accessed | tf_op | source)
XLA Modules:
  0.0 41.7 jit_solution(8642267313786384376)
XLA Ops:
  0.0 39.8 %shard_map.91 = bf16[128,2048]{1,0:T(8,128)(2,1)} custom-call(bf16[128,2048]{1,0:T(8,128)(2,1)} %bitcast.7, f32[1,128]{1,0:T(1,128)} %off_in.1, bf16[2048,512]{1,0:T(8,128)(2,1)} %qw_in.1, bf16[2048,128]{1,0:T(8,128)(2,1)} %kw_in.1, bf16[2048,128]{1,0:T(8,128)(2,1)} %vw_in.1, bf16[16,2048]{1,0:T(8,128)(2,1)} %bitcast.8, f32[1,16]{1,0:T(1,128)} %bitcast.10, ...), custom_call_target="tpu_custom_call" | custom-call | tf_op jit(solution)/shard_map/pallas_call | solution.py:585
  39.8 1.9 %copy.11 = bf16[1,128,2048]{2,1,0:T(8,128)(2,1)} copy(bf16[1,128,2048]{2,1,0:T(8,128)(2,1)} %bitcast.6) | data formatting | bytes 1048576

commit v5 on v4

--- a/solution.py
+++ b/solution.py
@@ -299,7 +299,21 @@
             barrier, inc=1, device_id={"sp": s + 1}, device_id_type=pl.DeviceIdType.MESH
         )
 
-    pl.semaphore_wait(barrier, seqs - 1 + (s + spread - 1) // spread + 1 - (s + 1) // spread)
+    @pl.when(s > 1)
+    def _():
+        pl.semaphore_signal(
+            barrier, inc=1, device_id={"sp": s - 2}, device_id_type=pl.DeviceIdType.MESH
+        )
+
+    @pl.when(s < spread - 2)
+    def _():
+        pl.semaphore_signal(
+            barrier, inc=1, device_id={"sp": s + 2}, device_id_type=pl.DeviceIdType.MESH
+        )
+
+    below = (s + spread - 1) // spread + (s + spread - 2) // spread
+    above = 2 - (s + 1) // spread - (s + 2) // spread
+    pl.semaphore_wait(barrier, seqs - 1 + below + above)
 
     load_tok.wait()
     part = pl.ds(pl.multiple_of(core * half, half), half)
@@ -330,11 +344,11 @@
 
     here = pl.ds(pl.multiple_of(s * rows, rows), rows)
 
-    def kv_copy(slot, block):
+    def kv_copy(slot, block, hop=1):
         piece = kv.at[slot, :, pl.ds(pl.multiple_of(block * rows, rows), rows)]
         return remote(
-            piece, piece, kv_send_sem.at[slot, block], kv_recv_sem.at[slot, block],
-            sp=(s + 1) % spread,
+            piece, piece, kv_send_sem.at[slot, hop - 1, block], kv_recv_sem.at[slot, block],
+            sp=(s + hop) % spread,
         )
 
     def gate_chain(block):
@@ -347,6 +361,10 @@
         pair = jnp.dot(tok[slot], kvw[...], preferred_element_type=jnp.float32)
         kv[slot, 0, here] = unit(pair[:, :head_dim])
         kv[slot, 1, here] = pair[:, head_dim:].astype(jnp.bfloat16)
+
+        @pl.when(s < spread - 2)
+        def _():
+            kv_copy(slot, s, 2).start()
 
         @pl.when(s < spread - 1)
         def _():
@@ -469,20 +487,29 @@
                 head_norm(mixed, OUT_FLOOR) * gain
             ).astype(jnp.bfloat16)
 
+    some = (s + spread - 1) // spread
+
+    def member(places):
+        if len(places) == spread:
+            return s >= 0
+        return last if places[0] == spread - 1 else s < spread - 1
+
     def finish(first, stop, places):
         def each(slot, carry):
             for known in range(first, stop):
-                if spread - 1 in places:
-
-                    @pl.when(jnp.logical_and(last, slot == known))
-                    def _():
-                        def arrive(k, inner):
-                            if known == 2:
+                @pl.when(jnp.logical_and(member(places), slot == known))
+                def _():
+                    def arrive(k, inner):
+                        if known == 2:
+
+                            @pl.when(last)
+                            def _():
                                 gate_chain(s - k).wait_recv()
-                            kv_copy(known, s - k).wait_recv()
-                            return inner
-
-                        lax.fori_loop(1, s + 1, arrive, 0)
+
+                        kv_copy(known, s - k).wait_recv()
+                        return inner
+
+                    lax.fori_loop(1, 1 + some + (s + 1) // spread * (s - some), arrive, 0)
 
             for k in places:
 
@@ -503,7 +530,6 @@
         lax.fori_loop(first, stop, each, 0)
 
     some = (s + spread - 1) // spread
-    relay(1, 1 + some, [0, 1])
     over[0].wait_recv()
     onward[0].start()
     for step in range(1, seqs):
@@ -519,7 +545,8 @@
     project_kv(2)
     project_q(1)
     relay(2, s + 1, [0, 1])
-    relay(1, s + 1, [2], True)
+    relay(1, s + 1, [], True)
+    relay(2, s + 1, [2])
     over[1].wait_recv()
     onward[1].start()
     project_q(2)
@@ -527,7 +554,6 @@
     project_kv(3)
     others = list(range(spread - 1))
     everywhere = list(range(spread))
-    relay(1, 1 + some, [3])
     finish(2, 3, everywhere)
     project_q(3)
     relay(2, s + 1, [3])
@@ -549,13 +575,23 @@
 
     @pl.when(s < spread - 1)
     def _():
+        def drain_gates(block, carry):
+            gate_chain(block).wait_send()
+            return carry
+
         def drain(block, carry):
-            gate_chain(block).wait_send()
             for slot in range(seqs):
                 kv_copy(slot, block).wait_send()
             return carry
 
-        lax.fori_loop(0, s + 1, drain, 0)
+        lax.fori_loop(0, s + 1, drain_gates, 0)
+        lax.fori_loop(0, s - 1, drain, 0)
+        drain(s, 0)
+
+    @pl.when(s < spread - 2)
+    def _():
+        for slot in range(seqs):
+            kv_copy(slot, s, 2).wait_send()
 
     store.wait()
 
@@ -603,7 +639,7 @@
             dma((5,)),
             dma((seqs,)),
             dma((seqs,)),
-            dma((seqs, spread)),
+            dma((seqs, 2, spread)),
             dma((seqs, spread)),
             dma((spread,)),
             dma((spread,)),

time: 41.9 us -> 43.9 us (1.048)
  Pallas kernels: 39.8 us -> 41.8 us
    pallas_call x1, Pallas kernels: 39.8 us -> 41.8 us  [fused(): pl.pallas_call(fused_kernel, out_shape=jax.ShapeDtypeStruct((rows, seqs *...]
where the time goes in v5:
time: 43.9 us; the launch traced here: 43.7 us
  Pallas kernels  41.8 us (95%)
  local copies, waits for them, and re-layouts  1.88 us (4%)
    pallas_call x1, Pallas kernels, fused(): pl.pallas_call(fused_kernel, out_shape=jax.ShapeDtypeStruct((rows, seqs *...  41.8 us
    unnamed x1, local copies, waits for them, and re-layouts  1.88 us

profile of v5, /device:TPU:25, one launch (start us, length us, event | category | flops | bytes accessed | tf_op | source)
XLA Modules:
  0.0 43.7 jit_solution(10856037798943973707)
XLA Ops:
  0.0 41.8 %shard_map.91 = bf16[128,2048]{1,0:T(8,128)(2,1)} custom-call(bf16[128,2048]{1,0:T(8,128)(2,1)} %bitcast.7, f32[1,128]{1,0:T(1,128)} %off_in.1, bf16[2048,512]{1,0:T(8,128)(2,1)} %qw_in.1, bf16[2048,128]{1,0:T(8,128)(2,1)} %kw_in.1, bf16[2048,128]{1,0:T(8,128)(2,1)} %vw_in.1, bf16[16,2048]{1,0:T(8,128)(2,1)} %bitcast.8, f32[1,16]{1,0:T(1,128)} %bitcast.10, ...), custom_call_target="tpu_custom_call" | custom-call | tf_op jit(solution)/shard_map/pallas_call | solution.py:621
  41.8 1.9 %copy.11 = bf16[1,128,2048]{2,1,0:T(8,128)(2,1)} copy(bf16[1,128,2048]{2,1,0:T(8,128)(2,1)} %bitcast.6) | data formatting | bytes 1048576

commit v6 on v4

--- a/solution.py
+++ b/solution.py
@@ -528,9 +528,9 @@
     others = list(range(spread - 1))
     everywhere = list(range(spread))
     relay(1, 1 + some, [3])
-    finish(2, 3, everywhere)
     project_q(3)
     relay(2, s + 1, [3])
+    finish(2, 3, everywhere)
     finish(0, 2, [spread - 1])
     finish(3, seqs, everywhere)
     finish(0, 2, others)

time: 41.9 us -> 41.3 us (0.986)
  Pallas kernels: 39.8 us -> 39.2 us
    pallas_call x1, Pallas kernels: 39.8 us -> 39.2 us  [fused(): pl.pallas_call(fused_kernel, out_shape=jax.ShapeDtypeStruct((rows, seqs *...]
where the time goes in v6:
time: 41.3 us; the launch traced here: 41.1 us
  Pallas kernels  39.2 us (95%)
  local copies, waits for them, and re-layouts  1.88 us (5%)
    pallas_call x1, Pallas kernels, fused(): pl.pallas_call(fused_kernel, out_shape=jax.ShapeDtypeStruct((rows, seqs *...  39.2 us
    unnamed x1, local copies, waits for them, and re-layouts  1.88 us

profile of v6, /device:TPU:25, one launch (start us, length us, event | category | flops | bytes accessed | tf_op | source)
XLA Modules:
  0.0 41.1 jit_solution(3396195851869292521)
XLA Ops:
  0.0 39.2 %shard_map.91 = bf16[128,2048]{1,0:T(8,128)(2,1)} custom-call(bf16[128,2048]{1,0:T(8,128)(2,1)} %bitcast.7, f32[1,128]{1,0:T(1,128)} %off_in.1, bf16[2048,512]{1,0:T(8,128)(2,1)} %qw_in.1, bf16[2048,128]{1,0:T(8,128)(2,1)} %kw_in.1, bf16[2048,128]{1,0:T(8,128)(2,1)} %vw_in.1, bf16[16,2048]{1,0:T(8,128)(2,1)} %bitcast.8, f32[1,16]{1,0:T(1,128)} %bitcast.10, ...), custom_call_target="tpu_custom_call" | custom-call | tf_op jit(solution)/shard_map/pallas_call | solution.py:585
  39.3 1.9 %copy.11 = bf16[1,128,2048]{2,1,0:T(8,128)(2,1)} copy(bf16[1,128,2048]{2,1,0:T(8,128)(2,1)} %bitcast.6) | data formatting | bytes 1048576
